TPU v7x, 32 devices: a whole 2x2x4 slice. The times are simulated.
32 devices in a mesh: ep: 8 (over z, y), tp: 4 (over x, core).
Axes of the slice: x: 2, y: 2, z: 4, core: 2. Of those that a mesh axis runs over, the one named last changes fastest.
Arguments:
- mixer_in: bfloat16 [3072, 2048], P(('ep', 'tp')), may hold values from -6 to 6
- expert_in: bfloat16 [3072, 2048], P(('ep', 'tp')), may hold values from -6 to 6
- mixer_gain: float32 [2048], replicated, may hold values from 0.1 to 1.9
- in_gate_weight: bfloat16 [2048, 2048], P(None, 'tp'), may hold values from -0.125 to 0.125
- out_gate_weight: bfloat16 [2048, 2048], P(None, 'tp'), may hold values from -0.125 to 0.125
- value_weight: bfloat16 [2048, 2048], P(None, 'tp'), may hold values from -0.125 to 0.125
- conv_taps: float32 [3, 2048], replicated, may hold values from -3 to 3
- mixer_proj: bfloat16 [2048, 2048], P(None, 'tp'), may hold values from -0.125 to 0.125
- expert_gain: float32 [2048], replicated, may hold values from 0.1 to 1.9
- route_ids: int32 [3072, 2], P('ep'), may hold values from 0 to 7, all different within a row; in each aligned block of 96 rows (0 to 95, 96 to 191, ...) at most 48 rows name the same one
- route_weights: float32 [3072, 2], P('ep'), may hold values from 0.1 to 1
- gate_weight: bfloat16 [8, 2048, 1024], P('ep', None, 'tp'), may hold values from -0.125 to 0.125
- up_weight: bfloat16 [8, 2048, 1024], P('ep', None, 'tp'), may hold values from -0.125 to 0.125
- down_weight: bfloat16 [8, 1024, 2048], P('ep', None, 'tp'), may hold values from -0.1875 to 0.1875
Outputs:
- mixer_out: bfloat16 [3072, 2048], P('ep', 'tp')
- expert_out: bfloat16 [3072, 2048], P('ep', 'tp')
Inputs may be any that keep to these rules, and one draw needn't show every extreme that they name: `route_ids`: each row names 2 different experts. In each aligned block of 96 rows no expert is named by more than 48 rows, a bound that some block reaches.
All inputs are finite; a program needn't handle non-finite values.
Results may differ from a plain program's by a relative error of at most 0.0076.
Values may be sent and summed in bfloat16 or wider, within the bound.
No kernel may reach another device: no remote copies, remote signals or barrier semaphores. Data moves between devices by JAX's collectives and lax.ppermute only.
A program may use at most 64 MiB of HBM per device.

v0:
```python
import jax
import jax.numpy as jnp
from jax import lax
from jax.sharding import PartitionSpec as P

norm_eps = 1e-06


def passed_along(value, axis, steps):
    count = lax.axis_size(axis)
    leading, last = (max(0, -steps), min(count, count - steps))
    return lax.ppermute(value, axis, [(source, source + steps) for source in range(leading, last)])


def rms_rows(values, gain_row):
    wide = values.astype(jnp.float32)
    scale = lax.rsqrt(jnp.mean(wide * wide, axis=-1, keepdims=True) + norm_eps)
    return (wide * scale * gain_row).astype(jnp.bfloat16)


def place_slots(route_ids, group_rows, experts, slot_cap):
    row_total, top_count = route_ids.shape
    groups = row_total // group_rows
    labels = jnp.arange(experts, dtype=jnp.int32)
    onehot = (
        route_ids.reshape(groups, group_rows * top_count)[:, :, None] == labels[None, None, :]
    ).astype(jnp.int32)
    earlier = jnp.cumsum(onehot, axis=1) - onehot
    within = jnp.sum(earlier * onehot, axis=2)
    slot_index = jnp.arange(groups, dtype=jnp.int32)[:, None] * slot_cap + within
    return slot_index.reshape(row_total, top_count)


def on_device(
    mixer_in,
    expert_in,
    mixer_gain,
    in_gate_weight,
    out_gate_weight,
    value_weight,
    conv_taps,
    mixer_proj,
    expert_gain,
    route_ids,
    route_weights,
    gate_weight,
    up_weight,
    down_weight,
):
    tok_dev = mixer_in.shape[0]
    tp_count = lax.axis_size("tp")
    ep_count = lax.axis_size("ep")
    top_count = route_ids.shape[1]
    experts = ep_count * gate_weight.shape[0]
    slot_cap = max(2, 2 * tok_dev * top_count // experts)
    tp_index = lax.axis_index("tp")
    mixer_normed = rms_rows(mixer_in, mixer_gain)
    expert_normed = rms_rows(expert_in, expert_gain)
    block_slot = place_slots(route_ids, tok_dev, experts, slot_cap)
    mixer_rows = lax.all_gather(mixer_normed, "tp", axis=0, tiled=True)
    send_ids = lax.dynamic_slice_in_dim(route_ids, tp_index * tok_dev, tok_dev, 0)
    send_slot = (
        lax.dynamic_slice_in_dim(block_slot, tp_index * tok_dev, tok_dev, 0) - tp_index * slot_cap
    )
    source_count = expert_normed.shape[0]
    flat_index = (send_ids * slot_cap + send_slot).reshape(-1)
    row_table = (
        jnp.full((experts * slot_cap,), source_count, jnp.int32)
        .at[flat_index]
        .set(jnp.repeat(jnp.arange(source_count, dtype=jnp.int32), top_count))
    )
    padded_rows = jnp.concatenate(
        [expert_normed, jnp.zeros((1, expert_normed.shape[1]), jnp.bfloat16)], axis=0
    )
    outgoing = padded_rows[row_table].reshape(experts, slot_cap, expert_normed.shape[1])
    arrived = lax.all_to_all(outgoing, "ep", split_axis=0, concat_axis=0, tiled=True)
    arrived = lax.all_gather(arrived, "tp", axis=1, tiled=True)
    chan_width = in_gate_weight.shape[1]
    in_gate = jnp.dot(mixer_rows, in_gate_weight, preferred_element_type=jnp.float32)
    out_gate = jnp.dot(mixer_rows, out_gate_weight, preferred_element_type=jnp.float32)
    values = jnp.dot(mixer_rows, value_weight, preferred_element_type=jnp.float32)
    product = (in_gate * values).astype(jnp.bfloat16)
    tap_count = conv_taps.shape[0]
    rim_rows = passed_along(product[product.shape[0] - (tap_count - 1) :], "ep", 1)
    extended = jnp.concatenate([rim_rows, product], axis=0).astype(jnp.float32)
    tap_rows = lax.dynamic_slice_in_dim(conv_taps, tp_index * chan_width, chan_width, 1)
    row_count = product.shape[0]
    conv_sum = tap_rows[0] * extended[0:row_count]
    for tap_index in range(1, tap_count):
        conv_sum = conv_sum + tap_rows[tap_index] * extended[tap_index : tap_index + row_count]
    gated = (out_gate * conv_sum).astype(jnp.bfloat16)
    slots_in = arrived.reshape(-1, arrived.shape[2])
    gate_pre = jnp.dot(slots_in, gate_weight[0], preferred_element_type=jnp.float32)
    up_pre = jnp.dot(slots_in, up_weight[0], preferred_element_type=jnp.float32)
    hidden = (jax.nn.silu(gate_pre) * up_pre).astype(jnp.bfloat16)
    down_slice = down_weight[0]
    gated_all, hidden_all = (
        lax.all_gather(gated, "tp", axis=1, tiled=True),
        lax.all_gather(hidden, "tp", axis=1, tiled=True),
    )
    mixer_sum = jnp.dot(gated_all, mixer_proj, preferred_element_type=jnp.float32)
    expert_sum = jnp.dot(hidden_all, down_slice, preferred_element_type=jnp.float32)
    mixer_out = mixer_sum.astype(jnp.bfloat16)
    results = expert_sum.astype(jnp.bfloat16).reshape(ep_count, -1, expert_sum.shape[1])
    returned = lax.all_to_all(results, "ep", split_axis=0, concat_axis=0, tiled=True)
    back_index = (route_ids * (tp_count * slot_cap) + block_slot).reshape(-1)
    picked = returned.reshape(-1, returned.shape[2])[back_index].reshape(
        route_ids.shape[0], top_count, -1
    )
    shares = route_weights / jnp.sum(route_weights, axis=1, keepdims=True)
    expert_out = jnp.sum(picked.astype(jnp.float32) * shares[:, :, None], axis=1).astype(
        jnp.bfloat16
    )
    return (mixer_out, expert_out)


def solution(mesh):
    return jax.shard_map(
        on_device,
        mesh=mesh,
        in_specs=(
            P(("ep", "tp"), None),
            P(("ep", "tp"), None),
            P(),
            P(None, "tp"),
            P(None, "tp"),
            P(None, "tp"),
            P(),
            P(None, "tp"),
            P(),
            P("ep", None),
            P("ep", None),
            P("ep", None, "tp"),
            P("ep", None, "tp"),
            P("ep", None, "tp"),
        ),
        out_specs=(P("ep", "tp"), P("ep", "tp")),
        check_vma=False,
    )
```

profile of v0, /device:TPU:0, one launch (start us, length us, event | category | flops | bytes accessed | tf_op | source)
XLA Modules:
  0.0 225.8 jit_solution(8903931806457454474)
XLA Ops:
  7.3 1.0 copy.26
  8.4 2.3 %reduce-window.6 = s32[4,8,2,128]{3,1,2,0:T(8,128)S(1)} reduce-window(s32[4,8,2,128]{3,1,2,0:T(8,128)S(1)} %convert_bitcast_fusion, s32[]{:T(128)} %constant.19.clone.1), window={size=1x1x1x128 pad=0_0x0_0x0_0x127_0}, to_apply=%region_2.0 | reduce-window | flops 1040384 | bytes 65540 | tf_op jit(solution)/shard_map/reduce-window
  11.0 0.2 reduce_sum.50
  11.5 0.7 multiply_add_fusion
  12.2 0.8 subtract_add_fusion
  13.3 1.2 scatter_custom_fusion
  14.6 0.2 fusion.10
  15.0 3.1 %gather_fusion = bf16[384,2048]{1,0:T(8,128)(2,1)} fusion(bf16[97,2048]{1,0:T(8,128)(2,1)S(1)} %concatenate.7, s32[1024]{0:T(1024)S(1)} %pad_clamp_fusion.1), kind=kCustom, calls=%fused_computation | custom fusion | bytes 3147264 | tf_op jit(solution)/shard_map/gather | solution.py:75
  18.1 44.4 %all_to_all.10 = bf16[8,48,2048]{2,1,0:T(8,128)(2,1)} all-to-all(bf16[8,48,2048]{2,1,0:T(8,128)(2,1)} %bitcast.37), channel_id=1, replica_groups=mesh['ep'=8,'tp'=4] {'ep'}, dimensions={0} | all-to-all | bytes 3145728 | tf_op jit(solution)/shard_map/all_to_all | solution.py:76
  62.6 0.9 copy-done.2
  63.5 0.2 fusion.7
  63.7 0.9 fusion.9
  64.7 43.4 %all-gather.9.cloned.1.call-done = bf16[8,192,2048]{2,1,0:T(8,128)(2,1)} async-done(((bf16[8,48,2048]{2,1,0:T(8,128)(2,1)}), bf16[8,192,2048]{2,1,0:T(8,128)(2,1)}) %all-gather.9.cloned.1.call-update) | async-done | bytes 6291472 | tf_op jit(solution)/shard_map/all_gather | solution.py:77
  108.1 4.8 %fusion.5 = f32[1536,256]{1,0:T(8,128)S(1)} fusion(bf16[1536,2048]{1,0:T(8,128)(2,1)} %bitcast.43, bf16[1,2048,256]{2,1,0:T(8,128)(2,1)S(1)} %copy-done.9), kind=kOutput, calls=%fused_computation.14 | convolution fusion | flops 1610612736 | bytes 8912896 | tf_op jit(solution)/shard_map/dot_general | solution.py:93
  112.9 3.0 %fusion = bf16[1536,256]{1,0:T(8,128)(2,1)} fusion(bf16[1536,2048]{1,0:T(8,128)(2,1)S(1)} %bitcast.44, f32[1536,256]{1,0:T(8,128)S(1)} %fusion.5, bf16[1,2048,256]{2,1,0:T(8,128)(2,1)S(1)} %copy-done.10), kind=kOutput, calls=%fused_computation.5 | convolution fusion | flops 1612972032 | bytes 9699328 | tf_op jit(solution)/shard_map/dot_general | solution.py:94
  115.9 14.0 %all-gather.5.cloned.1.call-done = bf16[384,2048]{1,0:T(8,128)(2,1)} async-done(((bf16[96,2048]{1,0:T(8,128)(2,1)}), bf16[384,2048]{1,0:T(8,128)(2,1)}) %all-gather.5.cloned.1.call-update) | async-done | bytes 1572880 | tf_op jit(solution)/shard_map/all_gather | solution.py:60
  129.9 2.5 %fusion.22 = f32[384,512]{1,0:T(8,128)S(1)} fusion(bf16[384,2048]{1,0:T(8,128)(2,1)} %all-gather.5.cloned.1.call-done, bf16[2048,512]{1,0:T(8,128)(2,1)S(1)} %copy-done), kind=kOutput, calls=%fused_computation.57 | convolution fusion | flops 805306368 | bytes 4456448 | tf_op jit(solution)/shard_map/dot_general | solution.py:79
  132.4 1.0 fusion.2
  133.4 3.4 %collective-permute-start = (bf16[2,512]{1,0:T(2,128)(2,1)S(1)}, bf16[2,512]{1,0:T(2,128)(2,1)S(1)}, u32[]{:S(2)}, u32[]{:S(2)}) collective-permute-start(bf16[2,512]{1,0:T(2,128)(2,1)S(1)} %slice.44), channel_id=1, source_target_pairs={{0,4},{4,8},{8,12},{12,16},{16,20},{20,24},{24,28},{1,5},{5,9},{9,... | collective-permute-start | bytes 6152 | tf_op jit(solution)/shard_map/ppermute | solution.py:12
  136.8 0.9 constant_dynamic-slice_fusion
  137.7 0.4 collective-permute-done
  138.2 22.1 %all-gather.11.cloned.1.call-done = bf16[1536,1024]{1,0:T(8,128)(2,1)} async-done(((bf16[1536,256]{1,0:T(8,128)(2,1)}), bf16[1536,1024]{1,0:T(8,128)(2,1)}) %all-gather.11.cloned.1.call-update) | async-done | bytes 3145744 | tf_op jit(solution)/shard_map/all_gather | solution.py:99
  160.3 5.1 %convolution_convert_fusion = bf16[1536,512]{1,0:T(8,128)(2,1)} fusion(bf16[1536,1024]{1,0:T(8,128)(2,1)} %all-gather.11.cloned.1.call-done, bf16[1,1024,512]{2,1,0:T(8,128)(2,1)} %param.27), kind=kOutput, calls=%fused_computation.3 | convolution fusion | flops 1611399168 | bytes 5767168 | tf_op jit(solution)/shard_map/dot_general | solution.py:102
  165.5 5.5 %all-to-all-start.1 = ((bf16[8,192,512]{2,1,0:T(8,128)(2,1)}), bf16[8,192,512]{2,1,0:T(8,128)(2,1)}, u32[]{:S(2)}, u32[]{:S(2)}) async-start(bf16[8,192,512]{2,1,0:T(8,128)(2,1)} %bitcast.38), calls=%async_computation.1 | async-start | bytes 3145728 | tf_op jit(solution)/shard_map/all_to_all | solution.py:105
  171.0 0.2 all-gather.7.cloned.1.call-start
  171.2 3.9 %fusion.1 = bf16[384,512]{1,0:T(8,128)(2,1)} fusion(bf16[384,2048]{1,0:T(8,128)(2,1)} %all-gather.5.cloned.1.call-done, bf16[2048,512]{1,0:T(8,128)(2,1)} %param.18, f32[386,512]{1,0:T(8,128)S(1)} %maximum_convert_fusion, f32[512]{0:T(512)S(1)} %bitcast.41, f32[512]{0:T(512)S(1)} %bitcast.40, f32[512]{0:T(512)S(1)} %bitcast.39), kind=kOutput, calls=%fused_computation.9 | convolution fusion | flops 806682624 | bytes 6428672 | tf_op jit(solution)/shard_map/dot_general | solution.py:80
  175.7 19.5 %all-gather.7.cloned.1.call-done = bf16[384,2048]{1,0:T(8,128)(2,1)} async-done(((bf16[384,512]{1,0:T(8,128)(2,1)}), bf16[384,2048]{1,0:T(8,128)(2,1)}) %all-gather.7.cloned.1.call-update) | async-done | bytes 1572880 | tf_op jit(solution)/shard_map/all_gather | solution.py:98
  195.2 3.8 %convolution_convert_fusion.1 = bf16[384,512]{1,0:T(8,128)(2,1)} fusion(bf16[384,2048]{1,0:T(8,128)(2,1)} %all-gather.7.cloned.1.call-done, bf16[2048,512]{1,0:T(8,128)(2,1)} %param.21), kind=kOutput, calls=%fused_computation.11 | convolution fusion | flops 805502976 | bytes 4063232 | tf_op jit(solution)/shard_map/dot_general | solution.py:101
  199.0 9.5 %all-to-all-done.1 = bf16[8,192,512]{2,1,0:T(8,128)(2,1)} async-done(((bf16[8,192,512]{2,1,0:T(8,128)(2,1)}), bf16[8,192,512]{2,1,0:T(8,128)(2,1)}, u32[]{:S(2)}, u32[]{:S(2)}) %all-to-all-start.1) | async-done | bytes 1572896 | tf_op jit(solution)/shard_map/all_to_all | solution.py:105
  208.5 4.3 %gather_fusion.1 = bf16[768,512]{1,0:T(8,128)(2,1)S(1)} fusion(bf16[1536,512]{1,0:T(8,128)(2,1)} %bitcast.14, s32[1024]{0:T(1024)S(1)} %pad_clamp_fusion), kind=kCustom, calls=%fused_computation.1 | custom fusion | bytes 1575936 | tf_op jit(solution)/shard_map/gather | solution.py:107
  212.8 2.1 reshape.134
  215.0 4.3 %multiply_reduce_fusion = bf16[384,512]{1,0:T(8,128)(2,1)} fusion(f32[384,2,512]{2,1,0:T(2,128)} %reshape.134, f32[384,2]{1,0:T(8,128)S(1)} %copy.32), kind=kLoop, calls=%fused_computation.6 | loop fusion | flops 589824 | bytes 1969152 | tf_op jit(solution)/shard_map/reduce_sum | solution.py:111
  (62 shorter events, 2.2 us)
Async XLA Ops:
  7.2 122.7 %copy-start = (bf16[2048,512]{1,0:T(8,128)(2,1)S(1)}, bf16[2048,512]{1,0:T(8,128)(2,1)}, u32[]{:S(2)}) copy-start(bf16[2048,512]{1,0:T(8,128)(2,1)} %param.17) | copy-start | bytes 6291460
  7.2 7.4 %copy-start.1 = (bf16[96,2048]{1,0:T(8,128)(2,1)S(1)}, bf16[96,2048]{1,0:T(8,128)(2,1)}, u32[]{:S(2)}) copy-start(bf16[96,2048]{1,0:T(8,128)(2,1)} %param.15) | copy-start | bytes 1179652
  7.2 7.6 %copy-start.4 = (f32[2048]{0:T(1024)S(1)}, f32[2048]{0:T(1024)}, u32[]{:S(2)}) copy-start(f32[2048]{0:T(1024)} %param.22) | copy-start | bytes 24580
  7.2 100.8 %all-gather.9.cloned.1.call-start = ((), (), s32[]{:S(2)}) async-start(), calls=%async_computation.4 | async-start | bytes 7864320 | tf_op jit(solution)/shard_map/all_gather | solution.py:77
  62.5 1.0 copy-start.2
  62.5 1.2 copy-start.5
  62.5 45.5 %copy-start.9 = (bf16[1,2048,256]{2,1,0:T(8,128)(2,1)S(1)}, bf16[1,2048,256]{2,1,0:T(8,128)(2,1)}, u32[]{:S(2)}) copy-start(bf16[1,2048,256]{2,1,0:T(8,128)(2,1)} %param.25) | copy-start | bytes 3145732
  62.5 67.3 %all-gather.5.cloned.1.call-start = ((), (), s32[]{:S(2)}) async-start(), calls=%async_computation.2 | async-start | bytes 1966080 | tf_op jit(solution)/shard_map/all_gather | solution.py:60
  64.6 95.7 %all-gather.11.cloned.1.call-start = ((), (), s32[]{:S(2)}) async-start(), calls=%async_computation.5 | async-start | bytes 3932160 | tf_op jit(solution)/shard_map/all_gather | solution.py:99
  108.0 4.8 %copy-start.6 = (bf16[8,192,2048]{2,1,0:T(8,128)(2,1)S(1)}, bf16[8,192,2048]{2,1,0:T(8,128)(2,1)}, u32[]{:S(2)}) copy-start(bf16[8,192,2048]{2,1,0:T(8,128)(2,1)} %all-gather.9.cloned.1.call-done) | copy-start | bytes 18874372
  108.1 4.9 %copy-start.10 = (bf16[1,2048,256]{2,1,0:T(8,128)(2,1)S(1)}, bf16[1,2048,256]{2,1,0:T(8,128)(2,1)}, u32[]{:S(2)}) copy-start(bf16[1,2048,256]{2,1,0:T(8,128)(2,1)} %param.26) | copy-start | bytes 3145732
  129.8 2.5 %copy-start.7 = (bf16[2048,512]{1,0:T(8,128)(2,1)S(1)}, bf16[2048,512]{1,0:T(8,128)(2,1)}, u32[]{:S(2)}) copy-start(bf16[2048,512]{1,0:T(8,128)(2,1)} %param.19) | copy-start | bytes 6291460
  129.9 2.5 %copy-start.8 = (bf16[384,2048]{1,0:T(8,128)(2,1)S(1)}, bf16[384,2048]{1,0:T(8,128)(2,1)}, u32[]{:S(2)}) copy-start(bf16[384,2048]{1,0:T(8,128)(2,1)} %all-gather.5.cloned.1.call-done) | copy-start | bytes 4718596
  133.4 4.7 %collective-permute-start = (bf16[2,512]{1,0:T(2,128)(2,1)S(1)}, bf16[2,512]{1,0:T(2,128)(2,1)S(1)}, u32[]{:S(2)}, u32[]{:S(2)}) collective-permute-start(bf16[2,512]{1,0:T(2,128)(2,1)S(1)} %slice.44), channel_id=1, source_target_pairs={{0,4},{4,8},{8,12},{12,16},{16,20},{20,24},{24,28},{1,5},{5,9},{9,... | collective-permute-start | bytes 6152 | tf_op jit(solution)/shard_map/ppermute | solution.py:12
  165.5 43.0 %all-to-all-start.1 = ((bf16[8,192,512]{2,1,0:T(8,128)(2,1)}), bf16[8,192,512]{2,1,0:T(8,128)(2,1)}, u32[]{:S(2)}, u32[]{:S(2)}) async-start(bf16[8,192,512]{2,1,0:T(8,128)(2,1)} %bitcast.38), calls=%async_computation.1 | async-start | bytes 3145728 | tf_op jit(solution)/shard_map/all_to_all | solution.py:105
  171.0 24.2 %all-gather.7.cloned.1.call-start = ((), (), s32[]{:S(2)}) async-start(), calls=%async_computation.3 | async-start | bytes 1966080 | tf_op jit(solution)/shard_map/all_gather | solution.py:98
  171.2 4.2 %copy-start.3 = (f32[384,2]{0,1:T(2,128)S(1)}, f32[384,2]{0,1:T(2,128)}, u32[]{:S(2)}) copy-start(f32[384,2]{0,1:T(2,128)} %param.24) | copy-start | bytes 9220
Sparse Core Ops, SparseCore 0:
  62.7 45.3 all-gather.8
  110.2 19.6 all-gather.4
  131.4 28.8 all-gather.10
  175.3 19.8 all-gather.6
where the time goes:
time: 226 us
  waiting for transfers between devices  109 us (48%)
  blocking collectives  44.4 us (20%)
  matrix products  24.1 us (11%)
  local copies, waits for them, and re-layouts  15.3 us (7%)
  between operations  14 us (6%)
  other arithmetic  9.84 us (4%)
  starting transfers between devices  9.23 us (4%)
    all_to_all x1, blocking collectives, on_device(): lax.all_to_all(outgoing, 'ep', split_axis=0, concat_axis=0, tiled=True)  44.4 us
    all_gather x1, waiting for transfers between devices, on_device(): arrived = lax.all_gather(arrived, 'tp', axis=1, tiled=True)  43.4 us
    all_gather x1, waiting for transfers between devices, on_device(): lax.all_gather(hidden, 'tp', axis=1, tiled=True)  22.1 us
    all_gather x1, waiting for transfers between devices, on_device(): lax.all_gather(gated, 'tp', axis=1, tiled=True)  19.5 us
    all_gather x1, waiting for transfers between devices, on_device(): mixer_rows = lax.all_gather(mixer_normed, 'tp', axis=0, tiled=True)  14 us
    all_to_all x1, waiting for transfers between devices, on_device(): lax.all_to_all(results, 'ep', split_axis=0, concat_axis=0, tiled=True)  9.53 us
    all_to_all x1, starting transfers between devices, on_device(): lax.all_to_all(results, 'ep', split_axis=0, concat_axis=0, tiled=True)  5.52 us
    dot_general x1, matrix products, on_device(): jnp.dot(hidden_all, down_slice, preferred_element_type=jnp.float32)  5.13 us
  transfers between devices with their start and end apart: 6, of which 6 were waited for; matrix products, arithmetic and copies ran while one was open for 10% of the time, Pallas kernels for 0%

commit v1 on v0

--- a/solution.py
+++ b/solution.py
@@ -74,7 +74,7 @@
     )
     outgoing = padded_rows[row_table].reshape(experts, slot_cap, expert_normed.shape[1])
     arrived = lax.all_to_all(outgoing, "ep", split_axis=0, concat_axis=0, tiled=True)
-    arrived = lax.all_gather(arrived, "tp", axis=1, tiled=True)
+    arrived = jnp.concatenate(lax.all_gather(arrived, "tp"), axis=1)
     chan_width = in_gate_weight.shape[1]
     in_gate = jnp.dot(mixer_rows, in_gate_weight, preferred_element_type=jnp.float32)
     out_gate = jnp.dot(mixer_rows, out_gate_weight, preferred_element_type=jnp.float32)

time: 226 us -> 226 us (level)
  local copies, waits for them, and re-layouts: 15.3 us -> 18.7 us
  matrix products: 24.1 us -> 21.2 us
    reshape x0 -> x1, local copies, waits for them, and re-layouts: none -> 3.45 us  [on_device(): arrived = jnp.concatenate(lax.all_gather(arrived, 'tp'), axis=1)]
    dot_general x1, matrix products: 4.78 us -> 1.91 us  [on_device(): jnp.dot(slots_in, gate_weight[0], preferred_element_type=jnp.float32)]
where the time goes in v1:
time: 226 us
  waiting for transfers between devices  108 us (48%)
  blocking collectives  44.4 us (20%)
  matrix products  21.2 us (9%)
  local copies, waits for them, and re-layouts  18.7 us (8%)
  between operations  14.1 us (6%)
  other arithmetic  9.84 us (4%)
  starting transfers between devices  9.23 us (4%)
    all_to_all x1, blocking collectives, on_device(): lax.all_to_all(outgoing, 'ep', split_axis=0, concat_axis=0, tiled=True)  44.4 us
    all_gather x1, waiting for transfers between devices, on_device(): arrived = jnp.concatenate(lax.all_gather(arrived, 'tp'), axis=1)  43.4 us
    all_gather x1, waiting for transfers between devices, on_device(): lax.all_gather(hidden, 'tp', axis=1, tiled=True)  22.1 us
    all_gather x1, waiting for transfers between devices, on_device(): lax.all_gather(gated, 'tp', axis=1, tiled=True)  19.5 us
    all_gather x1, waiting for transfers between devices, on_device(): mixer_rows = lax.all_gather(mixer_normed, 'tp', axis=0, tiled=True)  13.4 us
    all_to_all x1, waiting for transfers between devices, on_device(): lax.all_to_all(results, 'ep', split_axis=0, concat_axis=0, tiled=True)  9.53 us
    all_to_all x1, starting transfers between devices, on_device(): lax.all_to_all(results, 'ep', split_axis=0, concat_axis=0, tiled=True)  5.52 us
    dot_general x1, matrix products, on_device(): jnp.dot(hidden_all, down_slice, preferred_element_type=jnp.float32)  5.12 us
  transfers between devices with their start and end apart: 6, of which 6 were waited for; matrix products, arithmetic and copies ran while one was open for 10% of the time, Pallas kernels for 0%

profile of v1, /device:TPU:0, one launch (start us, length us, event | category | flops | bytes accessed | tf_op | source)
XLA Modules:
  0.0 225.8 jit_solution(11423715341642668984)
XLA Ops:
  7.3 1.0 copy.42
  8.4 2.3 %reduce-window.6 = s32[4,8,2,128]{3,1,2,0:T(8,128)S(1)} reduce-window(s32[4,8,2,128]{3,1,2,0:T(8,128)S(1)} %convert_bitcast_fusion, s32[]{:T(128)} %constant.19.clone.1), window={size=1x1x1x128 pad=0_0x0_0x0_0x127_0}, to_apply=%region_2.0 | reduce-window | flops 1040384 | bytes 65540 | tf_op jit(solution)/shard_map/reduce-window
  11.0 0.2 reduce_sum.50
  11.5 0.7 multiply_add_fusion
  12.2 0.8 subtract_add_fusion
  13.3 1.2 scatter_custom_fusion
  14.6 0.2 fusion.10
  15.0 3.1 %gather_fusion = bf16[384,2048]{1,0:T(8,128)(2,1)} fusion(bf16[97,2048]{1,0:T(8,128)(2,1)S(1)} %concatenate.7, s32[1024]{0:T(1024)S(1)} %pad_clamp_fusion.1), kind=kCustom, calls=%fused_computation | custom fusion | bytes 3147264 | tf_op jit(solution)/shard_map/gather | solution.py:75
  18.1 44.4 %all_to_all.10 = bf16[8,48,2048]{2,1,0:T(8,128)(2,1)} all-to-all(bf16[8,48,2048]{2,1,0:T(8,128)(2,1)} %bitcast.43), channel_id=1, replica_groups=mesh['ep'=8,'tp'=4] {'ep'}, dimensions={0} | all-to-all | bytes 3145728 | tf_op jit(solution)/shard_map/all_to_all | solution.py:76
  62.6 0.9 copy-done.2
  63.7 0.9 fusion.9
  64.7 43.4 %all-gather.12.cloned.1.call-done = bf16[32,48,2048]{2,1,0:T(8,128)(2,1)} async-done(((bf16[8,48,2048]{2,1,0:T(8,128)(2,1)}), bf16[32,48,2048]{2,1,0:T(8,128)(2,1)}) %all-gather.12.cloned.1.call-update) | async-done | bytes 6291472 | tf_op jit(solution)/shard_map/all_gather | solution.py:77
  108.1 3.5 %copy.47 = bf16[8,4,48,2048]{3,2,1,0:T(8,128)(2,1)S(1)} copy(bf16[8,4,48,2048]{3,2,0,1:T(8,128)(2,1)} %bitcast.40) | data formatting | bytes 12582912 | tf_op jit(solution)/shard_map/reshape | solution.py:77
  111.5 1.9 fusion.5
  113.5 3.0 %fusion = bf16[1536,256]{1,0:T(8,128)(2,1)} fusion(bf16[1536,2048]{1,0:T(8,128)(2,1)S(1)} %bitcast.42, f32[1536,256]{1,0:T(8,128)S(1)} %fusion.5, bf16[1,2048,256]{2,1,0:T(8,128)(2,1)S(1)} %copy-done.9), kind=kOutput, calls=%fused_computation.5 | convolution fusion | flops 1612972032 | bytes 9699328 | tf_op jit(solution)/shard_map/dot_general | solution.py:94
  116.5 13.4 %all-gather.6.cloned.1.call-done = bf16[384,2048]{1,0:T(8,128)(2,1)} async-done(((bf16[96,2048]{1,0:T(8,128)(2,1)}), bf16[384,2048]{1,0:T(8,128)(2,1)}) %all-gather.6.cloned.1.call-update) | async-done | bytes 1572880 | tf_op jit(solution)/shard_map/all_gather | solution.py:60
  129.9 2.5 %fusion.22 = f32[384,512]{1,0:T(8,128)S(1)} fusion(bf16[384,2048]{1,0:T(8,128)(2,1)} %all-gather.6.cloned.1.call-done, bf16[2048,512]{1,0:T(8,128)(2,1)S(1)} %copy-done), kind=kOutput, calls=%fused_computation.57 | convolution fusion | flops 805306368 | bytes 4456448 | tf_op jit(solution)/shard_map/dot_general | solution.py:79
  132.4 1.0 fusion.2
  133.4 3.4 %collective-permute-start = (bf16[2,512]{1,0:T(2,128)(2,1)S(1)}, bf16[2,512]{1,0:T(2,128)(2,1)S(1)}, u32[]{:S(2)}, u32[]{:S(2)}) collective-permute-start(bf16[2,512]{1,0:T(2,128)(2,1)S(1)} %slice.44), channel_id=1, source_target_pairs={{0,4},{4,8},{8,12},{12,16},{16,20},{20,24},{24,28},{1,5},{5,9},{9,... | collective-permute-start | bytes 6152 | tf_op jit(solution)/shard_map/ppermute | solution.py:12
  136.8 0.9 constant_dynamic-slice_fusion
  137.7 0.4 collective-permute-done
  138.2 22.1 %all-gather.10.cloned.1.call-done = bf16[1536,1024]{1,0:T(8,128)(2,1)} async-done(((bf16[1536,256]{1,0:T(8,128)(2,1)}), bf16[1536,1024]{1,0:T(8,128)(2,1)}) %all-gather.10.cloned.1.call-update) | async-done | bytes 3145744 | tf_op jit(solution)/shard_map/all_gather | solution.py:99
  160.3 5.1 %convolution_convert_fusion = bf16[1536,512]{1,0:T(8,128)(2,1)} fusion(bf16[1536,1024]{1,0:T(8,128)(2,1)} %all-gather.10.cloned.1.call-done, bf16[1,1024,512]{2,1,0:T(8,128)(2,1)} %param.27), kind=kOutput, calls=%fused_computation.3 | convolution fusion | flops 1611399168 | bytes 5767168 | tf_op jit(solution)/shard_map/dot_general | solution.py:102
  165.5 5.5 %all-to-all-start.1 = ((bf16[8,192,512]{2,1,0:T(8,128)(2,1)}), bf16[8,192,512]{2,1,0:T(8,128)(2,1)}, u32[]{:S(2)}, u32[]{:S(2)}) async-start(bf16[8,192,512]{2,1,0:T(8,128)(2,1)} %bitcast.44), calls=%async_computation.1 | async-start | bytes 3145728 | tf_op jit(solution)/shard_map/all_to_all | solution.py:105
  171.0 0.2 all-gather.8.cloned.1.call-start
  171.2 3.9 %fusion.1 = bf16[384,512]{1,0:T(8,128)(2,1)} fusion(bf16[384,2048]{1,0:T(8,128)(2,1)} %all-gather.6.cloned.1.call-done, bf16[2048,512]{1,0:T(8,128)(2,1)} %param.18, f32[386,512]{1,0:T(8,128)S(1)} %maximum_convert_fusion, f32[512]{0:T(512)S(1)} %bitcast.47, f32[512]{0:T(512)S(1)} %bitcast.46, f32[512]{0:T(512)S(1)} %bitcast.45), kind=kOutput, calls=%fused_computation.9 | convolution fusion | flops 806682624 | bytes 6428672 | tf_op jit(solution)/shard_map/dot_general | solution.py:80
  175.7 19.5 %all-gather.8.cloned.1.call-done = bf16[384,2048]{1,0:T(8,128)(2,1)} async-done(((bf16[384,512]{1,0:T(8,128)(2,1)}), bf16[384,2048]{1,0:T(8,128)(2,1)}) %all-gather.8.cloned.1.call-update) | async-done | bytes 1572880 | tf_op jit(solution)/shard_map/all_gather | solution.py:98
  195.2 3.8 %convolution_convert_fusion.1 = bf16[384,512]{1,0:T(8,128)(2,1)} fusion(bf16[384,2048]{1,0:T(8,128)(2,1)} %all-gather.8.cloned.1.call-done, bf16[2048,512]{1,0:T(8,128)(2,1)} %param.21), kind=kOutput, calls=%fused_computation.11 | convolution fusion | flops 805502976 | bytes 4063232 | tf_op jit(solution)/shard_map/dot_general | solution.py:101
  199.0 9.5 %all-to-all-done.1 = bf16[8,192,512]{2,1,0:T(8,128)(2,1)} async-done(((bf16[8,192,512]{2,1,0:T(8,128)(2,1)}), bf16[8,192,512]{2,1,0:T(8,128)(2,1)}, u32[]{:S(2)}, u32[]{:S(2)}) %all-to-all-start.1) | async-done | bytes 1572896 | tf_op jit(solution)/shard_map/all_to_all | solution.py:105
  208.5 4.3 %gather_fusion.1 = bf16[768,512]{1,0:T(8,128)(2,1)S(1)} fusion(bf16[1536,512]{1,0:T(8,128)(2,1)} %bitcast.16, s32[1024]{0:T(1024)S(1)} %pad_clamp_fusion), kind=kCustom, calls=%fused_computation.1 | custom fusion | bytes 1575936 | tf_op jit(solution)/shard_map/gather | solution.py:107
  212.8 2.1 reshape.134
  215.0 4.3 %multiply_reduce_fusion = bf16[384,512]{1,0:T(8,128)(2,1)} fusion(f32[384,2,512]{2,1,0:T(2,128)} %reshape.134, f32[384,2]{1,0:T(8,128)S(1)} %copy.49), kind=kLoop, calls=%fused_computation.6 | loop fusion | flops 589824 | bytes 1969152 | tf_op jit(solution)/shard_map/reduce_sum | solution.py:111
  (61 shorter events, 2.4 us)
Async XLA Ops:
  7.2 122.7 %copy-start = (bf16[2048,512]{1,0:T(8,128)(2,1)S(1)}, bf16[2048,512]{1,0:T(8,128)(2,1)}, u32[]{:S(2)}) copy-start(bf16[2048,512]{1,0:T(8,128)(2,1)} %param.17) | copy-start | bytes 6291460
  7.2 7.4 %copy-start.1 = (bf16[96,2048]{1,0:T(8,128)(2,1)S(1)}, bf16[96,2048]{1,0:T(8,128)(2,1)}, u32[]{:S(2)}) copy-start(bf16[96,2048]{1,0:T(8,128)(2,1)} %param.15) | copy-start | bytes 1179652
  7.2 7.6 %copy-start.4 = (f32[2048]{0:T(1024)S(1)}, f32[2048]{0:T(1024)}, u32[]{:S(2)}) copy-start(f32[2048]{0:T(1024)} %param.22) | copy-start | bytes 24580
  7.2 100.9 %all-gather.12.cloned.1.call-start = ((), (), s32[]{:S(2)}) async-start(), calls=%async_computation.5 | async-start | bytes 7864320 | tf_op jit(solution)/shard_map/all_gather | solution.py:77
  62.5 1.0 copy-start.2
  62.5 1.2 copy-start.5
  62.5 67.3 %all-gather.6.cloned.1.call-start = ((), (), s32[]{:S(2)}) async-start(), calls=%async_computation.2 | async-start | bytes 1966080 | tf_op jit(solution)/shard_map/all_gather | solution.py:60
  64.6 95.7 %all-gather.10.cloned.1.call-start = ((), (), s32[]{:S(2)}) async-start(), calls=%async_computation.4 | async-start | bytes 3932160 | tf_op jit(solution)/shard_map/all_gather | solution.py:99
  108.1 3.5 %copy-start.8 = (bf16[1,2048,256]{2,1,0:T(8,128)(2,1)S(1)}, bf16[1,2048,256]{2,1,0:T(8,128)(2,1)}, u32[]{:S(2)}) copy-start(bf16[1,2048,256]{2,1,0:T(8,128)(2,1)} %param.25) | copy-start | bytes 3145732
  111.5 1.9 copy-start.9
  129.9 2.5 %copy-start.6 = (bf16[2048,512]{1,0:T(8,128)(2,1)S(1)}, bf16[2048,512]{1,0:T(8,128)(2,1)}, u32[]{:S(2)}) copy-start(bf16[2048,512]{1,0:T(8,128)(2,1)} %param.19) | copy-start | bytes 6291460
  129.9 2.5 %copy-start.7 = (bf16[384,2048]{1,0:T(8,128)(2,1)S(1)}, bf16[384,2048]{1,0:T(8,128)(2,1)}, u32[]{:S(2)}) copy-start(bf16[384,2048]{1,0:T(8,128)(2,1)} %all-gather.6.cloned.1.call-done) | copy-start | bytes 4718596
  133.4 4.7 %collective-permute-start = (bf16[2,512]{1,0:T(2,128)(2,1)S(1)}, bf16[2,512]{1,0:T(2,128)(2,1)S(1)}, u32[]{:S(2)}, u32[]{:S(2)}) collective-permute-start(bf16[2,512]{1,0:T(2,128)(2,1)S(1)} %slice.44), channel_id=1, source_target_pairs={{0,4},{4,8},{8,12},{12,16},{16,20},{20,24},{24,28},{1,5},{5,9},{9,... | collective-permute-start | bytes 6152 | tf_op jit(solution)/shard_map/ppermute | solution.py:12
  165.5 43.0 %all-to-all-start.1 = ((bf16[8,192,512]{2,1,0:T(8,128)(2,1)}), bf16[8,192,512]{2,1,0:T(8,128)(2,1)}, u32[]{:S(2)}, u32[]{:S(2)}) async-start(bf16[8,192,512]{2,1,0:T(8,128)(2,1)} %bitcast.44), calls=%async_computation.1 | async-start | bytes 3145728 | tf_op jit(solution)/shard_map/all_to_all | solution.py:105
  171.0 24.2 %all-gather.8.cloned.1.call-start = ((), (), s32[]{:S(2)}) async-start(), calls=%async_computation.3 | async-start | bytes 1966080 | tf_op jit(solution)/shard_map/all_gather | solution.py:98
  171.2 4.2 %copy-start.3 = (f32[384,2]{0,1:T(2,128)S(1)}, f32[384,2]{0,1:T(2,128)}, u32[]{:S(2)}) copy-start(f32[384,2]{0,1:T(2,128)} %param.24) | copy-start | bytes 9220
Sparse Core Ops, SparseCore 0:
  62.7 45.3 all-gather.11
  110.2 19.6 all-gather.5
  131.4 28.8 all-gather.9
  175.3 19.8 all-gather.7
